TPU v7x, 32 devices: a whole 2x2x4 slice. The times are simulated.
32 devices in a mesh: rep: 2 (over x), fs: 8 (over z, y), tp: 2 (over core).
Axes of the slice: x: 2, y: 2, z: 4, core: 2. Of those that a mesh axis runs over, the one named last changes fastest.
Arguments:
- residual: bfloat16 [8192, 2048], P(('rep', 'fs', 'tp')), may hold values from -6 to 6
- mixer_gain: float32 [2048], replicated, may hold values from 0.1 to 1.9
- gating_proj: bfloat16 [2048, 2048], P('fs', 'tp'), may hold values from -0.125 to 0.125
- spatial_proj: bfloat16 [2048, 2048], P('fs', 'tp'), as said below
- spatial_gain: float32 [2048], replicated, may hold values from 0.1 to 1.9
- spatial_bias: float32 [2048], replicated, may hold values from -3 to 3
- spatial_mix: bfloat16 [32, 128, 128], replicated, may hold values from -0.5 to 0.5
- spatial_offset: float32 [32, 128], replicated, may hold values from 0.5 to 1.5
- mixer_out: bfloat16 [2048, 2048], P('tp', 'fs'), may hold values from -0.125 to 0.125
- channel_gain: float32 [2048], replicated, may hold values from 0.1 to 1.9
- gate_proj: bfloat16 [2048, 2816], P('fs', 'tp'), may hold values from -0.125 to 0.125
- up_proj: bfloat16 [2048, 2816], P('fs', 'tp'), may hold values from -0.125 to 0.125
- conv_taps: float32 [3, 2816], replicated, may hold values from -3.5 to 3.5
- down_proj: bfloat16 [2816, 2048], P('tp', 'fs'), may hold values from -0.109375 to 0.109375
Outputs:
- layer_out: bfloat16 [8192, 2048], P(('rep', 'fs', 'tp'))
Inputs may be any that keep to these rules, and one draw needn't show every extreme that they name: `spatial_proj`: entries are bounded in magnitude by 56 / sqrt(2048).
All inputs are finite; a program needn't handle non-finite values.
Results may differ from a plain program's by a relative error of at most 0.015.
Values may be sent and summed in bfloat16 or wider, within the bound.
A program may use at most 128 MiB of HBM per device.

v0:
```python
import jax
import jax.numpy as jnp
from jax import lax
from jax.sharding import PartitionSpec as P

HEAD = 64
GROUP = 2048
BLOCK = 128
SEGMENT = 64
KCONV = 3
SEQ_LEN = 256


def round_trip(value):
    return lax.optimization_barrier(value.astype(jnp.bfloat16)).astype(jnp.float32)


def rms_normed(value, gain):
    wide = value.astype(jnp.float32)
    scale = lax.rsqrt(jnp.mean(wide * wide, axis=-1, keepdims=True) + 1e-06)
    return (wide * scale * gain).astype(jnp.bfloat16)


def fold_pair(normed, pieces):
    first = jnp.dot(normed, pieces[0], preferred_element_type=jnp.float32)
    second = jnp.dot(normed, pieces[1], preferred_element_type=jnp.float32)
    return (first, second)


def on_device(
    residual,
    mixer_gain,
    gating_proj,
    spatial_proj,
    spatial_gain,
    spatial_bias,
    spatial_mix,
    spatial_offset,
    mixer_out,
    channel_gain,
    gate_proj,
    up_proj,
    conv_taps,
    down_proj,
):
    position = lax.axis_index("tp")
    rows = lax.all_gather(residual, "tp", axis=0, tiled=True)
    group_rows = rows.shape[0]
    normed = rms_normed(rows, mixer_gain)
    width = gating_proj.shape[1]
    gating, spatial = fold_pair(
        normed,
        (
            lax.all_gather(gating_proj, "fs", axis=0, tiled=True),
            lax.all_gather(spatial_proj, "fs", axis=0, tiled=True),
        ),
    )
    act_u = jax.nn.gelu(round_trip(gating))
    act_v = jax.nn.gelu(round_trip(spatial))
    total, squares = lax.psum((jnp.sum(act_v, axis=-1), jnp.sum(act_v * act_v, axis=-1)), "tp")
    mean = (total / GROUP)[:, None]
    var = (squares / GROUP)[:, None] - mean * mean
    gain_here = lax.dynamic_slice_in_dim(spatial_gain, position * width, width)
    bias_here = lax.dynamic_slice_in_dim(spatial_bias, position * width, width)
    vnorm = ((act_v - mean) * lax.rsqrt(var + 1e-05) * gain_here + bias_here).astype(jnp.bfloat16)
    heads_here = width // HEAD
    mix_here = lax.dynamic_slice_in_dim(spatial_mix, position * heads_here, heads_here, 0)
    offset_here = lax.dynamic_slice_in_dim(spatial_offset, position * heads_here, heads_here, 0)
    place = jnp.arange(BLOCK) // SEGMENT
    allowed = place[None, :] <= place[:, None]
    weights = jnp.where(allowed[None], mix_here, jnp.zeros_like(mix_here))
    blocks = vnorm.reshape(group_rows // BLOCK, BLOCK, heads_here, HEAD)
    mixed = jnp.einsum("hij,njhd->nihd", weights, blocks, preferred_element_type=jnp.float32)
    mixed = mixed + offset_here.T[None, :, :, None]
    gated = (act_u * mixed.reshape(group_rows, width)).astype(jnp.bfloat16)
    out_whole = lax.all_gather(mixer_out, "fs", axis=1, tiled=True)
    part = gated
    mixer_part = lax.psum_scatter(
        jnp.dot(part, out_whole, preferred_element_type=jnp.float32).astype(jnp.bfloat16),
        "tp",
        scatter_dimension=0,
        tiled=True,
    ).astype(jnp.float32)
    middle = (residual.astype(jnp.float32) + mixer_part).astype(jnp.bfloat16)
    rows2 = lax.all_gather(middle, "tp", axis=0, tiled=True)
    normed2 = rms_normed(rows2, channel_gain)
    units = gate_proj.shape[1]
    gate, up = fold_pair(
        normed2,
        (
            lax.all_gather(gate_proj, "fs", axis=0, tiled=True),
            lax.all_gather(up_proj, "fs", axis=0, tiled=True),
        ),
    )
    gate = round_trip(gate)
    up = round_trip(up)
    taps_here = lax.dynamic_slice_in_dim(conv_taps, position * units, units, 1)
    offset = jnp.arange(group_rows) % SEQ_LEN
    conv = taps_here[KCONV - 1] * gate
    for lag in range(1, KCONV):
        shifted = jnp.concatenate([jnp.zeros((lag, units), jnp.float32), gate[:-lag]], axis=0)
        shifted = jnp.where((offset >= lag)[:, None], shifted, 0.0)
        conv = conv + taps_here[KCONV - 1 - lag] * shifted
    hidden = (jax.nn.silu(conv) * up).astype(jnp.bfloat16)
    down_whole = lax.all_gather(down_proj, "fs", axis=1, tiled=True)
    part = hidden
    channel_part = lax.psum_scatter(
        jnp.dot(part, down_whole, preferred_element_type=jnp.float32).astype(jnp.bfloat16),
        "tp",
        scatter_dimension=0,
        tiled=True,
    ).astype(jnp.float32)
    return (middle.astype(jnp.float32) + channel_part).astype(jnp.bfloat16)


def solution(mesh):
    in_specs = (
        P(("rep", "fs", "tp"), None),
        P(),
        P("fs", "tp"),
        P("fs", "tp"),
        P(),
        P(),
        P(),
        P(),
        P("tp", "fs"),
        P(),
        P("fs", "tp"),
        P("fs", "tp"),
        P(),
        P("tp", "fs"),
    )
    out_specs = P(("rep", "fs", "tp"), None)
    return jax.shard_map(
        on_device, mesh=mesh, in_specs=in_specs, out_specs=out_specs, check_vma=False
    )
```

profile of v0, /device:TPU:0, one launch (start us, length us, event | category | flops | bytes accessed | tf_op | source)
XLA Modules:
  0.0 586.4 jit_solution(640272475224607658)
XLA Ops:
  6.5 0.0 copy-start
  6.5 0.0 all-gather.9.cloned.1.call-start
  6.5 0.7 all-gather.9.cloned.1.call-update
  7.3 0.0 copy-start.7
  7.3 0.0 all-gather.13.cloned.1.call-start
  7.3 0.7 all-gather.13.cloned.1.call-update
  8.0 0.0 all-gather.11.cloned.1.call-start
  8.1 0.7 all-gather.11.cloned.1.call-update
  8.8 0.0 all-gather.15.cloned.1.call-start
  8.8 0.5 all-gather.15.cloned.1.call-update
  9.3 0.0 reduce-scatter.3.cloned.1.call-start
  9.4 0.0 copy-done
  9.4 0.1 broadcast_compare_fusion
  9.5 12.7 %all-gather.9.cloned.1.call-done = bf16[512,2048]{1,0:T(8,128)(2,1)} async-done(((bf16[256,2048]{1,0:T(8,128)(2,1)}), bf16[512,2048]{1,0:T(8,128)(2,1)}) %all-gather.9.cloned.1.call-update) | async-done | bytes 2097168 | tf_op jit(solution)/shard_map/all_gather | solution.py:47
  22.2 2.2 fusion
  24.4 0.0 dynamic-slice-start
  24.5 0.0 dynamic-slice-start.1
  24.5 73.9 %all-gather.13.cloned.1.call-done = bf16[2048,1024]{1,0:T(8,128)(2,1)} async-done(((bf16[256,1024]{1,0:T(8,128)(2,1)}), bf16[2048,1024]{1,0:T(8,128)(2,1)}) %all-gather.13.cloned.1.call-update) | async-done | bytes 4194320 | tf_op jit(solution)/shard_map/all_gather | solution.py:55
  98.3 0.0 copy-done.7
  98.3 0.0 copy-done.4
  98.3 4.6 convolution_convert_fusion.4
  102.9 1.0 fusion.34
  103.9 2.5 all-reduce.2
  106.4 0.0 dynamic-slice-done
  106.4 0.0 dynamic-slice-done.1
  106.4 1.0 add_convert_fusion.2
  107.4 0.0 copy-start.6
  107.4 2.3 reshape.102
  109.7 0.0 copy-done.6
  109.7 2.6 bitcast_add_fusion
  112.4 3.0 copy.24
  115.3 3.5 reshape.103
  118.8 53.0 %all-gather.11.cloned.1.call-done = bf16[2048,1024]{1,0:T(8,128)(2,1)} async-done(((bf16[256,1024]{1,0:T(8,128)(2,1)}), bf16[2048,1024]{1,0:T(8,128)(2,1)}) %all-gather.11.cloned.1.call-update) | async-done | bytes 4194320 | tf_op jit(solution)/shard_map/all_gather | solution.py:54
  171.8 5.2 convolution_convert_fusion.5
  177.0 69.9 %all-gather.15.cloned.1.call-done = bf16[1024,2048]{1,0:T(8,128)(2,1)} async-done(((bf16[1024,256]{1,0:T(8,128)(2,1)}), bf16[1024,2048]{1,0:T(8,128)(2,1)}) %all-gather.15.cloned.1.call-update) | async-done | bytes 4194320 | tf_op jit(solution)/shard_map/all_gather | solution.py:76
  246.9 6.2 %convolution_convert_fusion = bf16[512,2048]{1,0:T(8,128)(2,1)} fusion(bf16[1024,2048]{1,0:T(8,128)(2,1)} %all-gather.15.cloned.1.call-done, f32[512,1024]{1,0:T(8,128)S(1)} %reshape.103, bf16[512,1024]{1,0:T(8,128)(2,1)S(1)} %convolution_convert_fusion.5), kind=kOutput, calls=%fused_computation.18 | convolution fusion | flops 2154299392 | bytes 9437184 | tf_op jit(solution)/shard_map/dot_general | solution.py:79
  253.1 0.0 reduce-scatter.3.cloned.1.call-update
  253.1 0.2 all-gather.17.cloned.1.call-start
  253.4 7.9 %reduce-scatter.3.cloned.1.call-done = bf16[256,2048]{1,0:T(8,128)(2,1)} async-done(((bf16[512,2048]{1,0:T(8,128)(2,1)}), bf16[256,2048]{1,0:T(8,128)(2,1)}) %reduce-scatter.3.cloned.1.call-update) | async-done | bytes 1048592 | tf_op jit(solution)/shard_map/reduce_scatter | solution.py:78
  261.2 2.6 add_convert_fusion.1
  263.8 0.0 all-gather.17.cloned.1.call-update
  263.8 0.0 all-gather.19.cloned.1.call-start
  263.9 0.7 all-gather.19.cloned.1.call-update
  264.6 0.0 all-gather.21.cloned.1.call-start
  264.6 0.7 all-gather.21.cloned.1.call-update
  265.3 0.0 all-gather.23.cloned.1.call-start
  265.4 0.7 all-gather.23.cloned.1.call-update
  266.1 0.0 reduce-scatter.5.cloned.1.call-start
  266.1 1.6 dynamic-slice_reduce_fusion.2
  267.7 0.5 fusion.47
  268.2 7.6 %all-gather.17.cloned.1.call-done = bf16[512,2048]{1,0:T(8,128)(2,1)} async-done(((bf16[256,2048]{1,0:T(8,128)(2,1)}), bf16[512,2048]{1,0:T(8,128)(2,1)}) %all-gather.17.cloned.1.call-update) | async-done | bytes 2097168 | tf_op jit(solution)/shard_map/all_gather | solution.py:85
  275.9 2.2 fusion.3
  278.1 93.5 %all-gather.19.cloned.1.call-done = bf16[2048,1408]{1,0:T(8,128)(2,1)} async-done(((bf16[256,1408]{1,0:T(8,128)(2,1)}), bf16[2048,1408]{1,0:T(8,128)(2,1)}) %all-gather.19.cloned.1.call-update) | async-done | bytes 5767184 | tf_op jit(solution)/shard_map/all_gather | solution.py:91
  371.6 6.1 %convolution_convert_fusion.2 = bf16[512,1408]{1,0:T(8,128)(2,1)S(1)} fusion(bf16[2048,1408]{1,0:T(8,128)(2,1)} %all-gather.19.cloned.1.call-done, bf16[512,2048]{1,0:T(8,128)(2,1)S(1)} %copy-done.5, f32[2048]{0:T(1024)} %param.23, f32[512]{0:T(512)S(1)} %add_rsqrt_fusion), kind=kOutput, calls=%fused_computation.20 | convolution fusion | flops 2957705216 | bytes 9316352 | tf_op jit(solution)/shard_map/dot_general | solution.py:25
  377.7 1.7 slice.20
  379.4 1.8 slice.21
  381.2 83.0 %all-gather.21.cloned.1.call-done = bf16[2048,1408]{1,0:T(8,128)(2,1)} async-done(((bf16[256,1408]{1,0:T(8,128)(2,1)}), bf16[2048,1408]{1,0:T(8,128)(2,1)}) %all-gather.21.cloned.1.call-update) | async-done | bytes 5767184 | tf_op jit(solution)/shard_map/all_gather | solution.py:92
  464.3 7.3 %convolution_convert_fusion.1 = bf16[512,1408]{1,0:T(8,128)(2,1)} fusion(bf16[2048,1408]{1,0:T(8,128)(2,1)} %all-gather.21.cloned.1.call-done, bf16[512,2048]{1,0:T(8,128)(2,1)S(1)} %copy-done.5, f32[2048]{0:T(1024)} %param.23, f32[512]{0:T(512)S(1)} %add_rsqrt_fusion), kind=kOutput, calls=%fused_computation.19 | convolution fusion | flops 2957705216 | bytes 9316352 | tf_op jit(solution)/shard_map/dot_general | solution.py:26
  471.6 86.1 %all-gather.23.cloned.1.call-done = bf16[1408,2048]{1,0:T(8,128)(2,1)} async-done(((bf16[1408,256]{1,0:T(8,128)(2,1)}), bf16[1408,2048]{1,0:T(8,128)(2,1)}) %all-gather.23.cloned.1.call-update) | async-done | bytes 5767184 | tf_op jit(solution)/shard_map/all_gather | solution.py:105
  557.7 11.1 %convolution_convert_fusion.3 = bf16[512,2048]{1,0:T(8,128)(2,1)} fusion(bf16[1408,2048]{1,0:T(8,128)(2,1)} %all-gather.23.cloned.1.call-done, bf16[512,1408]{1,0:T(8,128)(2,1)} %convolution_convert_fusion.1, f32[510,1408]{1,0:T(8,128)} %slice.21, f32[511,1408]{1,0:T(8,128)} %slice.20, f32[1408]{0:T(1024)} %get-tuple-element.9, f32[1408]{0:T(1024)} %get-tuple-element.8, ...), kind=kOutput, calls=%fused_computation.21 | convolution fusion | flops 2964652032 | bytes 16516096 | tf_op jit(solution)/shard_map/dot_general | solution.py:108
  568.8 0.0 reduce-scatter.5.cloned.1.call-update
  568.8 0.0 copy-start.1
  568.8 8.1 %reduce-scatter.5.cloned.1.call-done = bf16[256,2048]{1,0:T(8,128)(2,1)} async-done(((bf16[512,2048]{1,0:T(8,128)(2,1)}), bf16[256,2048]{1,0:T(8,128)(2,1)}) %reduce-scatter.5.cloned.1.call-update) | async-done | bytes 1048592 | tf_op jit(solution)/shard_map/reduce_scatter | solution.py:107
  576.9 2.6 add_convert_fusion
  (15 shorter events, 0.1 us)
Async XLA Ops:
  6.5 2.9 copy-start
  6.5 15.7 %all-gather.9.cloned.1.call-start = ((), (), s32[]{:S(2)}) async-start(), calls=%async_computation.2 | async-start | bytes 3145728 | tf_op jit(solution)/shard_map/all_gather | solution.py:47
  7.3 91.1 %copy-start.7 = (f32[2048]{0:T(1024)S(1)}, f32[2048]{0:T(1024)}, u32[]{:S(2)}) copy-start(f32[2048]{0:T(1024)} %param.15) | copy-start | bytes 24580
  7.3 91.1 %all-gather.13.cloned.1.call-start = ((), (), s32[]{:S(2)}) async-start(), calls=%async_computation.4 | async-start | bytes 4718592 | tf_op jit(solution)/shard_map/all_gather | solution.py:55
  8.0 163.8 %all-gather.11.cloned.1.call-start = ((), (), s32[]{:S(2)}) async-start(), calls=%async_computation.3 | async-start | bytes 4718592 | tf_op jit(solution)/shard_map/all_gather | solution.py:54
  8.8 238.2 %all-gather.15.cloned.1.call-start = ((), (), s32[]{:S(2)}) async-start(), calls=%async_computation.5 | async-start | bytes 4718592 | tf_op jit(solution)/shard_map/all_gather | solution.py:76
  9.3 251.9 %reduce-scatter.3.cloned.1.call-start = ((), (), s32[]{:S(2)}) async-start(), calls=%async_computation.6 | async-start | bytes 3145728 | tf_op jit(solution)/shard_map/reduce_scatter | solution.py:78
  22.2 76.1 %copy-start.4 = (bf16[512,2048]{1,0:T(8,128)(2,1)S(1)}, bf16[512,2048]{1,0:T(8,128)(2,1)}, u32[]{:S(2)}) copy-start(bf16[512,2048]{1,0:T(8,128)(2,1)} %all-gather.9.cloned.1.call-done) | copy-start | bytes 6291460
  24.4 81.9 %dynamic-slice-start = ((f32[2048]{0:T(1024)}, s32[]{:T(128)}), f32[1024]{0:T(1024)S(1)}, s32[]{:S(2)}) async-start(f32[2048]{0:T(1024)} %param.18, s32[]{:T(128)} %select_n.51), calls=%async_computation.12 | async-start | bytes 8704 | tf_op jit(solution)/shard_map/dynamic_slice | solution.py:63
  24.5 81.9 %dynamic-slice-start.1 = ((f32[2048]{0:T(1024)}, s32[]{:T(128)}), f32[1024]{0:T(1024)S(1)}, s32[]{:S(2)}) async-start(f32[2048]{0:T(1024)} %param.19, s32[]{:T(128)} %select_n.51), calls=%async_computation.13 | async-start | bytes 8704 | tf_op jit(solution)/shard_map/dynamic_slice | solution.py:64
  107.4 2.3 copy-start.6
  253.1 8.1 %copy-start.3 = (bf16[256,2048]{1,0:T(8,128)(2,1)S(1)}, bf16[256,2048]{1,0:T(8,128)(2,1)}, u32[]{:S(2)}) copy-start(bf16[256,2048]{1,0:T(8,128)(2,1)} %param.14) | copy-start | bytes 3145732
  253.1 22.7 %all-gather.17.cloned.1.call-start = ((), (), s32[]{:S(2)}) async-start(), calls=%async_computation.7 | async-start | bytes 3145728 | tf_op jit(solution)/shard_map/all_gather | solution.py:85
  263.8 107.7 %all-gather.19.cloned.1.call-start = ((), (), s32[]{:S(2)}) async-start(), calls=%async_computation.8 | async-start | bytes 6488064 | tf_op jit(solution)/shard_map/all_gather | solution.py:91
  264.6 199.7 %all-gather.21.cloned.1.call-start = ((), (), s32[]{:S(2)}) async-start(), calls=%async_computation.9 | async-start | bytes 6488064 | tf_op jit(solution)/shard_map/all_gather | solution.py:92
  265.3 292.3 %all-gather.23.cloned.1.call-start = ((), (), s32[]{:S(2)}) async-start(), calls=%async_computation.10 | async-start | bytes 6488064 | tf_op jit(solution)/shard_map/all_gather | solution.py:105
  266.1 310.8 %reduce-scatter.5.cloned.1.call-start = ((), (), s32[]{:S(2)}) async-start(), calls=%async_computation.11 | async-start | bytes 3145728 | tf_op jit(solution)/shard_map/reduce_scatter | solution.py:107
  275.9 95.7 %copy-start.5 = (bf16[512,2048]{1,0:T(8,128)(2,1)S(1)}, bf16[512,2048]{1,0:T(8,128)(2,1)}, u32[]{:S(2)}) copy-start(bf16[512,2048]{1,0:T(8,128)(2,1)} %all-gather.17.cloned.1.call-done) | copy-start | bytes 6291460
  381.2 176.4 %copy-start.8 = (pred[512]{0:T(512)(128)(4,1)S(1)}, pred[512]{0:T(512)(128)(4,1)}, u32[]{:S(2)}) copy-start(pred[512]{0:T(512)(128)(4,1)} %get-tuple-element.14) | copy-start | bytes 1540
  568.8 8.1 %copy-start.2 = (bf16[256,2048]{1,0:T(8,128)(2,1)S(1)}, bf16[256,2048]{1,0:T(8,128)(2,1)}, u32[]{:S(2)}) copy-start(bf16[256,2048]{1,0:T(8,128)(2,1)} %add_convert_fusion.1) | copy-start | bytes 3145732
  568.8 10.7 %copy-start.1 = (f32[32,128]{1,0:T(8,128)S(1)}, f32[32,128]{1,0:T(8,128)}, u32[]{:S(2)}) copy-start(f32[32,128]{1,0:T(8,128)} %param.21) | copy-start | bytes 49156
Sparse Core Ops, SparseCore 0:
  8.9 13.2 all-gather.8
  24.3 73.9 all-gather.12
  100.5 71.3 all-gather.10
  173.7 73.1 all-gather.14
  253.3 7.9 reduce-scatter.2
  264.0 11.8 all-gather.16
  278.0 93.4 all-gather.18
  373.7 90.4 all-gather.20
  466.3 91.3 all-gather.22
  569.0 7.9 reduce-scatter.4
where the time goes:
time: 587 us; the launch traced here: 586 us
  waiting for transfers between devices  500 us (85%)
  matrix products  43.1 us (7%)
  local copies, waits for them, and re-layouts  14 us (2%)
  between operations  13.7 us (2%)
  other arithmetic  12.2 us (2%)
    all_gather x1, waiting for transfers between devices, on_device(): lax.all_gather(gate_proj, 'fs', axis=0, tiled=True)  93.5 us
    all_gather x1, waiting for transfers between devices, on_device(): down_whole = lax.all_gather(down_proj, 'fs', axis=1, tiled=True)  86.1 us
    all_gather x1, waiting for transfers between devices, on_device(): lax.all_gather(up_proj, 'fs', axis=0, tiled=True)  83 us
    all_gather x1, waiting for transfers between devices, on_device(): lax.all_gather(spatial_proj, 'fs', axis=0, tiled=True)  73.9 us
    all_gather x1, waiting for transfers between devices, on_device(): out_whole = lax.all_gather(mixer_out, 'fs', axis=1, tiled=True)  69.9 us
    all_gather x1, waiting for transfers between devices, on_device(): lax.all_gather(gating_proj, 'fs', axis=0, tiled=True)  53 us
    all_gather x1, waiting for transfers between devices, on_device(): rows = lax.all_gather(residual, 'tp', axis=0, tiled=True)  12.7 us
    dot_general x2, matrix products, fold_pair(): second = jnp.dot(normed, pieces[1], preferred_element_type=jnp.float32)  11.9 us
  transfers between devices with their start and end apart: 10, of which 10 were waited for; matrix products, arithmetic and copies ran while one was open for 8% of the time, Pallas kernels for 0%

commit v1 on v0

--- a/solution.py
+++ b/solution.py
@@ -1,3 +1,4 @@
+import functools
 import jax
 import jax.numpy as jnp
 from jax import lax
@@ -9,6 +10,24 @@
 SEGMENT = 64
 KCONV = 3
 SEQ_LEN = 256
+
+
+def knots_mark(v0, mesh_name):
+    degree = lax.axis_size(mesh_name)
+    blocks_here = [v0]
+    for p in range(degree - 1):
+        blocks_here.append(
+            lax.ppermute(
+                blocks_here[-1], mesh_name, [(tick, (tick + 1) % degree) for tick in range(degree)]
+            )
+        )
+    clean = jnp.roll(
+        jnp.concatenate(blocks_here[::-1], 1), (lax.axis_index(mesh_name) + 1) * v0.shape[1], 1
+    )
+    return clean
+
+
+_list_members_all = functools.partial(knots_mark, mesh_name="fs")
 
 
 def round_trip(value):
@@ -102,7 +121,7 @@
         shifted = jnp.where((offset >= lag)[:, None], shifted, 0.0)
         conv = conv + taps_here[KCONV - 1 - lag] * shifted
     hidden = (jax.nn.silu(conv) * up).astype(jnp.bfloat16)
-    down_whole = lax.all_gather(down_proj, "fs", axis=1, tiled=True)
+    down_whole = _list_members_all(down_proj)
     part = hidden
     channel_part = lax.psum_scatter(
         jnp.dot(part, down_whole, preferred_element_type=jnp.float32).astype(jnp.bfloat16),

time: 587 us -> 567 us (0.966)
  waiting for transfers between devices: 500 us -> 457 us
  local copies, waits for them, and re-layouts: 14 us -> 35.3 us
    ppermute x0 -> x7, waiting for transfers between devices: none -> 204 us  [knots_mark(): lax.ppermute(blocks_here[-1], mesh_name, [(tick, (tick + 1) % degree) for...]
    all_gather x1, waiting for transfers between devices: 93.5 us -> 0.02 us  [on_device(): lax.all_gather(gate_proj, 'fs', axis=0, tiled=True)]
    all_gather x1 -> x0, waiting for transfers between devices: 86.1 us -> none  [on_device(): down_whole = lax.all_gather(down_proj, 'fs', axis=1, tiled=True)]
    all_gather x1, waiting for transfers between devices: 83 us -> 26.1 us  [on_device(): lax.all_gather(up_proj, 'fs', axis=0, tiled=True)]
    unnamed x18 -> x43, local copies, waits for them, and re-layouts: 0.04 us -> 20.9 us
    all_gather x1, waiting for transfers between devices: 7.65 us -> 0.01 us  [on_device(): rows2 = lax.all_gather(middle, 'tp', axis=0, tiled=True)]
  transfers between devices with their start and end apart: 10 -> 16, of which waited for: 10 -> 14; matrix products, arithmetic and copies ran while one was open for 8% -> 11% of each run, Pallas kernels for 0% -> 0%
where the time goes in v1:
time: 567 us; the launch traced here: 566 us
  waiting for transfers between devices  457 us (81%)
  matrix products  43.6 us (8%)
  local copies, waits for them, and re-layouts  35.3 us (6%)
  between operations  13.4 us (2%)
  other arithmetic  11.4 us (2%)
    ppermute x7, waiting for transfers between devices, knots_mark(): lax.ppermute(blocks_here[-1], mesh_name, [(tick, (tick + 1) % degree) for...  204 us
    all_gather x1, waiting for transfers between devices, on_device(): lax.all_gather(spatial_proj, 'fs', axis=0, tiled=True)  74 us
    all_gather x1, waiting for transfers between devices, on_device(): out_whole = lax.all_gather(mixer_out, 'fs', axis=1, tiled=True)  68.9 us
    all_gather x1, waiting for transfers between devices, on_device(): lax.all_gather(gating_proj, 'fs', axis=0, tiled=True)  52.2 us
    all_gather x1, waiting for transfers between devices, on_device(): lax.all_gather(up_proj, 'fs', axis=0, tiled=True)  26.1 us
    unnamed x43, local copies, waits for them, and re-layouts  20.9 us
    dot_general x2, matrix products, fold_pair(): first = jnp.dot(normed, pieces[0], preferred_element_type=jnp.float32)  12.9 us
    all_gather x1, waiting for transfers between devices, on_device(): rows = lax.all_gather(residual, 'tp', axis=0, tiled=True)  12.7 us
  transfers between devices with their start and end apart: 16, of which 14 were waited for; matrix products, arithmetic and copies ran while one was open for 11% of the time, Pallas kernels for 0%

profile of v1, /device:TPU:0, one launch (start us, length us, event | category | flops | bytes accessed | tf_op | source)
XLA Modules:
  0.0 566.0 jit_solution(15447162905289532325)
XLA Ops:
  6.5 0.7 all-gather.8.cloned.1.call-update
  7.3 0.0 all-gather.12.cloned.1.call-start
  7.3 0.7 all-gather.12.cloned.1.call-update
  8.1 0.7 all-gather.10.cloned.1.call-update
  8.8 0.5 all-gather.14.cloned.1.call-update
  9.3 0.0 reduce-scatter.3.cloned.1.call-start
  9.4 0.1 broadcast_compare_fusion
  9.5 12.7 %all-gather.8.cloned.1.call-done = bf16[512,2048]{1,0:T(8,128)(2,1)} async-done(((bf16[256,2048]{1,0:T(8,128)(2,1)}), bf16[512,2048]{1,0:T(8,128)(2,1)}) %all-gather.8.cloned.1.call-update) | async-done | bytes 2097168 | tf_op jit(solution)/shard_map/all_gather | solution.py:66
  22.2 2.1 fusion.2
  24.3 74.0 %all-gather.12.cloned.1.call-done = bf16[2048,1024]{1,0:T(8,128)(2,1)} async-done(((bf16[256,1024]{1,0:T(8,128)(2,1)}), bf16[2048,1024]{1,0:T(8,128)(2,1)}) %all-gather.12.cloned.1.call-update) | async-done | bytes 4194320 | tf_op jit(solution)/shard_map/all_gather | solution.py:74
  98.3 5.2 convolution_convert_fusion.3
  103.5 1.0 fusion.39
  104.5 2.6 all-reduce.2
  107.1 1.0 add_convert_fusion.2
  108.2 2.3 reshape.102
  110.5 2.6 bitcast_add_fusion
  113.1 3.0 copy.24
  116.1 3.5 reshape.103
  119.6 52.2 %all-gather.10.cloned.1.call-done = bf16[2048,1024]{1,0:T(8,128)(2,1)} async-done(((bf16[256,1024]{1,0:T(8,128)(2,1)}), bf16[2048,1024]{1,0:T(8,128)(2,1)}) %all-gather.10.cloned.1.call-update) | async-done | bytes 4194320 | tf_op jit(solution)/shard_map/all_gather | solution.py:73
  171.8 6.2 %convolution_convert_fusion.4 = bf16[512,1024]{1,0:T(8,128)(2,1)} fusion(bf16[2048,1024]{1,0:T(8,128)(2,1)} %all-gather.10.cloned.1.call-done, bf16[512,2048]{1,0:T(8,128)(2,1)} %all-gather.8.cloned.1.call-done, f32[2048]{0:T(1024)S(1)} %copy-done.12, f32[512]{0:T(512)S(1)} %add_rsqrt_fusion.2), kind=kOutput, calls=%fused_computation.45 | convolution fusion | flops 2152202240 | bytes 7350272 | tf_op jit(solution)/shard_map/dot_general | solution.py:44
  178.0 68.9 %all-gather.14.cloned.1.call-done = bf16[1024,2048]{1,0:T(8,128)(2,1)} async-done(((bf16[1024,256]{1,0:T(8,128)(2,1)}), bf16[1024,2048]{1,0:T(8,128)(2,1)}) %all-gather.14.cloned.1.call-update) | async-done | bytes 4194320 | tf_op jit(solution)/shard_map/all_gather | solution.py:95
  246.9 6.5 %convolution_convert_fusion = bf16[512,2048]{1,0:T(8,128)(2,1)} fusion(bf16[1024,2048]{1,0:T(8,128)(2,1)} %all-gather.14.cloned.1.call-done, f32[512,1024]{1,0:T(8,128)S(1)} %reshape.103, bf16[512,1024]{1,0:T(8,128)(2,1)} %convolution_convert_fusion.4), kind=kOutput, calls=%fused_computation.20 | convolution fusion | flops 2154299392 | bytes 9437184 | tf_op jit(solution)/shard_map/dot_general | solution.py:98
  253.5 0.2 all-gather.16.cloned.1.call-start
  253.7 7.9 %reduce-scatter.3.cloned.1.call-done = bf16[256,2048]{1,0:T(8,128)(2,1)} async-done(((bf16[512,2048]{1,0:T(8,128)(2,1)}), bf16[256,2048]{1,0:T(8,128)(2,1)}) %reduce-scatter.3.cloned.1.call-update) | async-done | bytes 1048592 | tf_op jit(solution)/shard_map/reduce_scatter | solution.py:97
  261.5 2.6 add_convert_fusion.1
  264.2 0.0 all-gather.18.cloned.1.call-start
  264.2 0.7 all-gather.18.cloned.1.call-update
  265.0 1.9 collective-permute-start
  266.9 0.0 reduce-scatter.5.cloned.1.call-start
  266.9 19.1 %collective-permute-done = bf16[1408,256]{1,0:T(8,128)(2,1)S(1)} collective-permute-done((bf16[1408,256]{1,0:T(8,128)(2,1)S(1)}, bf16[1408,256]{1,0:T(8,128)(2,1)S(1)}, u32[]{:S(2)}, u32[]{:S(2)}) %collective-permute-start) | collective-permute-done | bytes 720928 | tf_op jit(solution)/shard_map/ppermute | solution.py:20
  286.1 34.5 %collective-permute-done.1 = bf16[1408,256]{1,0:T(8,128)(2,1)S(1)} collective-permute-done((bf16[1408,256]{1,0:T(8,128)(2,1)S(1)}, bf16[1408,256]{1,0:T(8,128)(2,1)S(1)}, u32[]{:S(2)}, u32[]{:S(2)}) %collective-permute-start.1) | collective-permute-done | bytes 720928 | tf_op jit(solution)/shard_map/ppermute | solution.py:20
  320.6 26.9 %collective-permute-done.2 = bf16[1408,256]{1,0:T(8,128)(2,1)S(1)} collective-permute-done((bf16[1408,256]{1,0:T(8,128)(2,1)S(1)}, bf16[1408,256]{1,0:T(8,128)(2,1)S(1)}, u32[]{:S(2)}, u32[]{:S(2)}) %collective-permute-start.2) | collective-permute-done | bytes 720928 | tf_op jit(solution)/shard_map/ppermute | solution.py:20
  347.5 35.5 %collective-permute-done.3 = bf16[1408,256]{1,0:T(8,128)(2,1)S(1)} collective-permute-done((bf16[1408,256]{1,0:T(8,128)(2,1)S(1)}, bf16[1408,256]{1,0:T(8,128)(2,1)S(1)}, u32[]{:S(2)}, u32[]{:S(2)}) %collective-permute-start.3) | collective-permute-done | bytes 720928 | tf_op jit(solution)/shard_map/ppermute | solution.py:20
  383.0 0.9 copy-done.7
  383.9 35.3 %collective-permute-done.4 = bf16[1408,256]{1,0:T(8,128)(2,1)S(1)} collective-permute-done((bf16[1408,256]{1,0:T(8,128)(2,1)S(1)}, bf16[1408,256]{1,0:T(8,128)(2,1)S(1)}, u32[]{:S(2)}, u32[]{:S(2)}) %collective-permute-start.4) | collective-permute-done | bytes 720928 | tf_op jit(solution)/shard_map/ppermute | solution.py:20
  419.2 0.9 copy-done.9
  420.0 17.9 %collective-permute-done.5 = bf16[1408,256]{1,0:T(8,128)(2,1)} collective-permute-done((bf16[1408,256]{1,0:T(8,128)(2,1)S(1)}, bf16[1408,256]{1,0:T(8,128)(2,1)}, u32[]{:S(2)}, u32[]{:S(2)}) %collective-permute-start.5) | collective-permute-done | bytes 720928 | tf_op jit(solution)/shard_map/ppermute | solution.py:20
  438.0 1.0 dynamic-slice_reduce_fusion.2
  438.9 34.8 %collective-permute-done.6 = bf16[1408,256]{1,0:T(8,128)(2,1)} collective-permute-done((bf16[1408,256]{1,0:T(8,128)(2,1)}, bf16[1408,256]{1,0:T(8,128)(2,1)}, u32[]{:S(2)}, u32[]{:S(2)}) %collective-permute-start.6) | collective-permute-done | bytes 720928 | tf_op jit(solution)/shard_map/ppermute | solution.py:20
  473.7 2.1 constant_dynamic-update-slice_fusion.15
  475.8 2.1 constant_dynamic-update-slice_fusion.14
  477.9 1.0 constant_dynamic-update-slice_fusion.13
  478.9 1.0 constant_dynamic-update-slice_fusion.12
  479.9 1.0 constant_dynamic-update-slice_fusion.11
  480.9 1.0 constant_dynamic-update-slice_fusion.10
  481.9 1.0 constant_dynamic-update-slice_fusion.9
  482.8 1.0 constant_dynamic-update-slice_fusion.8
  483.8 2.1 constant_dynamic-update-slice_fusion.7
  485.9 2.1 constant_dynamic-update-slice_fusion.6
  488.0 1.0 constant_dynamic-update-slice_fusion.5
  489.0 0.9 constant_dynamic-update-slice_fusion.4
  489.9 1.0 constant_dynamic-update-slice_fusion.3
  490.9 1.0 constant_dynamic-update-slice_fusion.2
  491.8 1.0 constant_dynamic-update-slice_fusion.1
  492.8 1.0 constant_dynamic-update-slice_fusion
  493.8 2.1 fusion.5
  495.9 6.7 %convolution_convert_fusion.2 = bf16[512,1408]{1,0:T(8,128)(2,1)S(1)} fusion(bf16[2048,1408]{1,0:T(8,128)(2,1)} %all-gather.18.cloned.1.call-done, bf16[512,2048]{1,0:T(8,128)(2,1)} %all-gather.16.cloned.1.call-done, f32[2048]{0:T(1024)S(1)} %copy-done.13, f32[512]{0:T(512)S(1)} %add_rsqrt_fusion), kind=kOutput, calls=%fused_computation.23 | convolution fusion | flops 2957705216 | bytes 9316352 | tf_op jit(solution)/shard_map/dot_general | solution.py:44
  502.7 1.8 slice.21
  504.4 1.8 slice.20
  506.2 26.1 %all-gather.20.cloned.1.call-done = bf16[2048,1408]{1,0:T(8,128)(2,1)} async-done(((bf16[256,1408]{1,0:T(8,128)(2,1)}), bf16[2048,1408]{1,0:T(8,128)(2,1)}) %all-gather.20.cloned.1.call-update) | async-done | bytes 5767184 | tf_op jit(solution)/shard_map/all_gather | solution.py:111
  532.3 6.9 %convolution_convert_fusion.1 = bf16[512,1408]{1,0:T(8,128)(2,1)S(1)} fusion(bf16[2048,1408]{1,0:T(8,128)(2,1)} %all-gather.20.cloned.1.call-done, bf16[512,2048]{1,0:T(8,128)(2,1)} %all-gather.16.cloned.1.call-done, f32[2048]{0:T(1024)S(1)} %copy-done.13, f32[512]{0:T(512)S(1)} %add_rsqrt_fusion), kind=kOutput, calls=%fused_computation.22 | convolution fusion | flops 2957705216 | bytes 9316352 | tf_op jit(solution)/shard_map/dot_general | solution.py:45
  539.2 9.5 %fusion.8 = bf16[512,2048]{1,0:T(8,128)(2,1)} fusion(bf16[1408,4096]{1,0:T(8,128)(2,1)} %constant_dynamic-update-slice_fusion, s32[]{:T(128)S(6)} %select_n.72, bf16[512,1408]{1,0:T(8,128)(2,1)S(1)} %convolution_convert_fusion.1, f32[510,1408]{1,0:T(8,128)S(1)} %copy-done.4, f32[511,1408]{1,0:T(8,128)S(1)} %copy-done.5, f32[1408]{0:T(1024)S(1)} %get-tuple-element.9, ...), kind=kOutput, calls=%fused_computation.21 | convolution fusion | flops 2964652032 | bytes 16516100 | tf_op jit(solution)/shard_map/dot_general | solution.py:127
  548.8 8.1 %reduce-scatter.5.cloned.1.call-done = bf16[256,2048]{1,0:T(8,128)(2,1)} async-done(((bf16[512,2048]{1,0:T(8,128)(2,1)}), bf16[256,2048]{1,0:T(8,128)(2,1)}) %reduce-scatter.5.cloned.1.call-update) | async-done | bytes 1048592 | tf_op jit(solution)/shard_map/reduce_scatter | solution.py:126
  556.9 2.6 add_convert_fusion
  (52 shorter events, 0.3 us)
Async XLA Ops:
  6.5 2.9 copy-start
  6.5 91.8 %copy-start.12 = (f32[2048]{0:T(1024)S(1)}, f32[2048]{0:T(1024)}, u32[]{:S(2)}) copy-start(f32[2048]{0:T(1024)} %param.15) | copy-start | bytes 24580
  6.5 15.7 %all-gather.8.cloned.1.call-start = ((), (), s32[]{:S(2)}) async-start(), calls=%async_computation.2 | async-start | bytes 3145728 | tf_op jit(solution)/shard_map/all_gather | solution.py:66
  7.3 91.1 %all-gather.12.cloned.1.call-start = ((), (), s32[]{:S(2)}) async-start(), calls=%async_computation.4 | async-start | bytes 4718592 | tf_op jit(solution)/shard_map/all_gather | solution.py:74
  8.0 163.8 %all-gather.10.cloned.1.call-start = ((), (), s32[]{:S(2)}) async-start(), calls=%async_computation.3 | async-start | bytes 4718592 | tf_op jit(solution)/shard_map/all_gather | solution.py:73
  8.7 238.2 %all-gather.14.cloned.1.call-start = ((), (), s32[]{:S(2)}) async-start(), calls=%async_computation.5 | async-start | bytes 4718592 | tf_op jit(solution)/shard_map/all_gather | solution.py:95
  9.3 252.2 %reduce-scatter.3.cloned.1.call-start = ((), (), s32[]{:S(2)}) async-start(), calls=%async_computation.6 | async-start | bytes 3145728 | tf_op jit(solution)/shard_map/reduce_scatter | solution.py:97
  24.3 82.8 %dynamic-slice-start = ((f32[2048]{0:T(1024)}, s32[]{:T(128)}), f32[1024]{0:T(1024)S(1)}, s32[]{:S(2)}) async-start(f32[2048]{0:T(1024)} %param.19, s32[]{:T(128)} %select_n.63), calls=%async_computation.11 | async-start | bytes 8704 | tf_op jit(solution)/shard_map/dynamic_slice | solution.py:83
  24.3 82.8 %dynamic-slice-start.1 = ((f32[2048]{0:T(1024)}, s32[]{:T(128)}), f32[1024]{0:T(1024)S(1)}, s32[]{:S(2)}) async-start(f32[2048]{0:T(1024)} %param.18, s32[]{:T(128)} %select_n.63), calls=%async_computation.12 | async-start | bytes 8704 | tf_op jit(solution)/shard_map/dynamic_slice | solution.py:82
  104.5 6.0 %copy-start.11 = (bf16[32,128,128]{2,1,0:T(8,128)(2,1)S(1)}, bf16[32,128,128]{2,1,0:T(8,128)(2,1)}, u32[]{:S(2)}) copy-start(bf16[32,128,128]{2,1,0:T(8,128)(2,1)} %param.20) | copy-start | bytes 3145732
  178.0 83.6 %copy-start.3 = (bf16[256,2048]{1,0:T(8,128)(2,1)S(1)}, bf16[256,2048]{1,0:T(8,128)(2,1)}, u32[]{:S(2)}) copy-start(bf16[256,2048]{1,0:T(8,128)(2,1)} %param.14) | copy-start | bytes 3145732
  253.4 11.5 %copy-start.6 = (bf16[1408,256]{1,0:T(8,128)(2,1)S(1)}, bf16[1408,256]{1,0:T(8,128)(2,1)}, u32[]{:S(2)}) copy-start(bf16[1408,256]{1,0:T(8,128)(2,1)} %param.27) | copy-start | bytes 2162692
  253.5 240.3 %all-gather.16.cloned.1.call-start = ((), (), s32[]{:S(2)}) async-start(), calls=%async_computation.7 | async-start | bytes 3145728 | tf_op jit(solution)/shard_map/all_gather | solution.py:104
  264.2 231.7 %all-gather.18.cloned.1.call-start = ((), (), s32[]{:S(2)}) async-start(), calls=%async_computation.8 | async-start | bytes 6488064 | tf_op jit(solution)/shard_map/all_gather | solution.py:110
  264.9 267.4 %all-gather.20.cloned.1.call-start = ((), (), s32[]{:S(2)}) async-start(), calls=%async_computation.9 | async-start | bytes 6488064 | tf_op jit(solution)/shard_map/all_gather | solution.py:111
  265.0 21.1 %collective-permute-start = (bf16[1408,256]{1,0:T(8,128)(2,1)S(1)}, bf16[1408,256]{1,0:T(8,128)(2,1)S(1)}, u32[]{:S(2)}, u32[]{:S(2)}) collective-permute-start(bf16[1408,256]{1,0:T(8,128)(2,1)S(1)} %copy-done.6), channel_id=1, source_target_pairs={{0,2},{2,4},{4,6},{6,8},{8,10},{10,12},{12,14},{14,0},{1,3},{3,5},... | collective-permute-start | bytes 2162696 | tf_op jit(solution)/shard_map/ppermute | solution.py:20
  266.9 290.0 %reduce-scatter.5.cloned.1.call-start = ((), (), s32[]{:S(2)}) async-start(), calls=%async_computation.10 | async-start | bytes 3145728 | tf_op jit(solution)/shard_map/reduce_scatter | solution.py:126
  286.1 34.5 %collective-permute-start.1 = (bf16[1408,256]{1,0:T(8,128)(2,1)S(1)}, bf16[1408,256]{1,0:T(8,128)(2,1)S(1)}, u32[]{:S(2)}, u32[]{:S(2)}) collective-permute-start(bf16[1408,256]{1,0:T(8,128)(2,1)S(1)} %collective-permute-done), channel_id=1, source_target_pairs={{0,2},{2,4},{4,6},{6,8},{8,10},{10,12},{12,14},{14,0},{1,3},{3,5},... | collective-permute-start | bytes 2162696 | tf_op jit(solution)/shard_map/ppermute | solution.py:20
  320.6 26.9 %collective-permute-start.2 = (bf16[1408,256]{1,0:T(8,128)(2,1)S(1)}, bf16[1408,256]{1,0:T(8,128)(2,1)S(1)}, u32[]{:S(2)}, u32[]{:S(2)}) collective-permute-start(bf16[1408,256]{1,0:T(8,128)(2,1)S(1)} %collective-permute-done.1), channel_id=1, source_target_pairs={{0,2},{2,4},{4,6},{6,8},{8,10},{10,12},{12,14},{14,0},{1,3},{3,5},... | collective-permute-start | bytes 2162696 | tf_op jit(solution)/shard_map/ppermute | solution.py:20
  347.5 35.5 %collective-permute-start.3 = (bf16[1408,256]{1,0:T(8,128)(2,1)S(1)}, bf16[1408,256]{1,0:T(8,128)(2,1)S(1)}, u32[]{:S(2)}, u32[]{:S(2)}) collective-permute-start(bf16[1408,256]{1,0:T(8,128)(2,1)S(1)} %collective-permute-done.2), channel_id=1, source_target_pairs={{0,2},{2,4},{4,6},{6,8},{8,10},{10,12},{12,14},{14,0},{1,3},{3,5},... | collective-permute-start | bytes 2162696 | tf_op jit(solution)/shard_map/ppermute | solution.py:20
  383.0 0.9 copy-start.7
  383.9 35.3 %collective-permute-start.4 = (bf16[1408,256]{1,0:T(8,128)(2,1)S(1)}, bf16[1408,256]{1,0:T(8,128)(2,1)S(1)}, u32[]{:S(2)}, u32[]{:S(2)}) collective-permute-start(bf16[1408,256]{1,0:T(8,128)(2,1)S(1)} %collective-permute-done.3), channel_id=1, source_target_pairs={{0,2},{2,4},{4,6},{6,8},{8,10},{10,12},{12,14},{14,0},{1,3},{3,5},... | collective-permute-start | bytes 2162696 | tf_op jit(solution)/shard_map/ppermute | solution.py:20
  419.2 0.9 copy-start.9
  420.0 17.9 %collective-permute-start.5 = (bf16[1408,256]{1,0:T(8,128)(2,1)S(1)}, bf16[1408,256]{1,0:T(8,128)(2,1)}, u32[]{:S(2)}, u32[]{:S(2)}) collective-permute-start(bf16[1408,256]{1,0:T(8,128)(2,1)S(1)} %collective-permute-done.4), channel_id=1, source_target_pairs={{0,2},{2,4},{4,6},{6,8},{8,10},{10,12},{12,14},{14,0},{1,3},{3,5},... | collective-permute-start | bytes 2162696 | tf_op jit(solution)/shard_map/ppermute | solution.py:20
  437.9 35.8 %collective-permute-start.6 = (bf16[1408,256]{1,0:T(8,128)(2,1)}, bf16[1408,256]{1,0:T(8,128)(2,1)}, u32[]{:S(2)}, u32[]{:S(2)}) collective-permute-start(bf16[1408,256]{1,0:T(8,128)(2,1)} %collective-permute-done.5), channel_id=1, source_target_pairs={{0,2},{2,4},{4,6},{6,8},{8,10},{10,12},{12,14},{14,0},{1,3},{3,5},... | collective-permute-start | bytes 2162696 | tf_op jit(solution)/shard_map/ppermute | solution.py:20
  437.9 40.0 %copy-start.10 = (bf16[1408,256]{1,0:T(8,128)(2,1)S(1)}, bf16[1408,256]{1,0:T(8,128)(2,1)}, u32[]{:S(2)}) copy-start(bf16[1408,256]{1,0:T(8,128)(2,1)} %copy-done.9) | copy-start | bytes 2162692
  437.9 41.0 %copy-start.8 = (bf16[1408,256]{1,0:T(8,128)(2,1)S(1)}, bf16[1408,256]{1,0:T(8,128)(2,1)}, u32[]{:S(2)}) copy-start(bf16[1408,256]{1,0:T(8,128)(2,1)} %copy-done.7) | copy-start | bytes 2162692
  490.9 5.1 copy-start.13
  532.3 6.9 %copy-start.4 = (f32[510,1408]{1,0:T(8,128)S(1)}, f32[510,1408]{1,0:T(8,128)}, u32[]{:S(2)}) copy-start(f32[510,1408]{1,0:T(8,128)} %slice.21) | copy-start | bytes 8616964
  532.3 6.9 %copy-start.5 = (f32[511,1408]{1,0:T(8,128)S(1)}, f32[511,1408]{1,0:T(8,128)}, u32[]{:S(2)}) copy-start(f32[511,1408]{1,0:T(8,128)} %slice.20) | copy-start | bytes 8633860
  539.2 17.7 %copy-start.2 = (bf16[256,2048]{1,0:T(8,128)(2,1)S(1)}, bf16[256,2048]{1,0:T(8,128)(2,1)}, u32[]{:S(2)}) copy-start(bf16[256,2048]{1,0:T(8,128)(2,1)} %add_convert_fusion.1) | copy-start | bytes 3145732
  539.2 20.2 %copy-start.1 = (f32[32,128]{1,0:T(8,128)S(1)}, f32[32,128]{1,0:T(8,128)}, u32[]{:S(2)}) copy-start(f32[32,128]{1,0:T(8,128)} %param.21) | copy-start | bytes 49156
Sparse Core Ops, SparseCore 0:
  8.9 13.2 all-gather.7
  24.3 73.9 all-gather.11
  100.5 71.3 all-gather.9
  173.7 73.1 all-gather.13
  253.6 7.9 reduce-scatter.2
  264.3 11.8 all-gather.15
  278.3 134.3 all-gather.17
  414.9 117.3 all-gather.19
  548.9 7.9 reduce-scatter.4
